TPU v7x, 32 devices: a whole 2x2x4 slice. The times are simulated.
32 devices in a mesh: sp: 8 (over z, y), tp: 4 (over x, core).
Axes of the slice: x: 2, y: 2, z: 4, core: 2. Of those that a mesh axis runs over, the one named last changes fastest.
Arguments:
- hidden_in: bfloat16 [6144, 4096], P('sp', 'tp'), may hold values from -16 to 16
- norm_gain: bfloat16 [2, 4096], P(None, 'tp'), may hold values from 0.099609375 to 1.8984375
- value_proj: bfloat16 [2, 4096, 1024], P(None, 'tp', 'sp'), may hold values from -0.09375 to 0.09375
- gate_proj: bfloat16 [2, 4096, 1024], P(None, 'tp', 'sp'), may hold values from -0.09375 to 0.09375
- conv_taps: bfloat16 [2, 31, 1024], P(None, None, 'tp'), may hold values from -1 to 1
- conv_bias: bfloat16 [2, 1024], P(None, 'tp'), may hold values from -3 to 3
- group_gain: bfloat16 [2, 1024], P(None, 'tp'), may hold values from 0.099609375 to 1.8984375
- group_shift: bfloat16 [2, 1024], P(None, 'tp'), may hold values from -3 to 3
- out_proj: bfloat16 [2, 1024, 4096], P(None, 'sp', 'tp'), may hold values from -0.1875 to 0.1875
Outputs:
- hidden_out: bfloat16 [6144, 4096], P('sp', 'tp')
All inputs are finite; a program needn't handle non-finite values.
Results may differ from a plain program's by a relative error of at most 0.012.
Values may be sent and summed in bfloat16 or wider, within the bound.
A program may use at most 128 MiB of HBM per device.

v0:
```python
import jax
import jax.numpy as jnp
from jax import lax
from jax.sharding import PartitionSpec as P

D = 4096
C = 1024
GROUPS = 4
WIDTH = 31


row_floor = 1e-06
group_floor = 1e-05


def passed_along(value, axis, steps):
    count = lax.axis_size(axis)
    initial, last = (max(0, -steps), min(count, count - steps))
    return lax.ppermute(value, axis, [(source, source + steps) for source in range(initial, last)])


def rms_normed(residual_rows, gain_part):
    wide_rows = residual_rows.astype(jnp.float32)
    squares = lax.psum(jnp.sum(wide_rows * wide_rows, axis=1), "tp")
    scale_rows = lax.rsqrt(squares / D + row_floor)
    return (wide_rows * scale_rows[:, None] * gain_part.astype(jnp.float32)[None, :]).astype(
        jnp.bfloat16
    )


def gated_input(normed_rows, w_value, w_gate):
    numbers = (((0,), (1,)), ((), ()))
    value_part = lax.dot_general(w_value, normed_rows, numbers, preferred_element_type=jnp.float32)
    gate_part = lax.dot_general(w_gate, normed_rows, numbers, preferred_element_type=jnp.float32)
    summed = lax.psum_scatter(
        jnp.stack([value_part, gate_part], axis=1).astype(jnp.bfloat16),
        "tp",
        scatter_dimension=0,
        tiled=True,
    ).astype(jnp.float32)
    return (summed[:, 0] * jax.nn.sigmoid(summed[:, 1])).astype(jnp.bfloat16)


def depthwise(extended, taps_part, bias_part, out_len):
    widened = extended.astype(jnp.float32)
    taps = taps_part.astype(jnp.float32)
    filtered = (
        jnp.zeros((extended.shape[0], out_len), jnp.float32)
        + bias_part.astype(jnp.float32)[:, None]
    )
    for offset in range(WIDTH):
        filtered = filtered + taps[offset][:, None] * widened[:, offset : offset + out_len]
    return filtered


def group_normed(filtered, gain_part, shift_part, group_size):
    channels, out_len = filtered.shape
    grouped = filtered.reshape(channels // group_size, group_size, out_len)
    group_mean = jnp.mean(grouped, axis=1, keepdims=True)
    centered = grouped - group_mean
    group_var = jnp.mean(centered * centered, axis=1, keepdims=True)
    scaled = (centered * lax.rsqrt(group_var + group_floor)).reshape(channels, out_len)
    scaled = (
        scaled * gain_part.astype(jnp.float32)[:, None] + shift_part.astype(jnp.float32)[:, None]
    )
    return jax.nn.silu(scaled).astype(jnp.bfloat16)


def project_out(mixed, w_out):
    return lax.dot_general(
        lax.all_gather(mixed, "tp", axis=0, tiled=True),
        w_out,
        (((0,), (0,)), ((), ())),
        preferred_element_type=jnp.float32,
    )


def on_device(
    hidden_in,
    norm_gain,
    value_proj,
    gate_proj,
    conv_taps,
    conv_bias,
    group_gain,
    group_shift,
    out_proj,
):
    tok_rows = hidden_in.shape[0]
    layers = norm_gain.shape[0]
    reach_back = WIDTH - 1
    group_size = C // GROUPS
    all_value, all_gate, all_out = (
        lax.all_gather(value_proj, "sp", axis=2, tiled=True),
        lax.all_gather(gate_proj, "sp", axis=2, tiled=True),
        lax.all_gather(out_proj, "sp", axis=1, tiled=True),
    )
    residual_rows = hidden_in
    for level in range(layers):
        w_value, w_gate, w_out = (all_value[level], all_gate[level], all_out[level])
        normed_rows = rms_normed(residual_rows, norm_gain[level])
        gated = gated_input(normed_rows, w_value, w_gate)
        before = passed_along(gated[:, tok_rows - reach_back :], "sp", 1)
        extended = jnp.concatenate([before, gated], axis=1)
        out_len = extended.shape[1] - reach_back
        filtered = depthwise(extended, conv_taps[level], conv_bias[level], out_len)
        mixed = group_normed(filtered, group_gain[level], group_shift[level], group_size)
        update = project_out(mixed, w_out)
        kept_rows = residual_rows
        residual_rows = (kept_rows.astype(jnp.float32) + update).astype(jnp.bfloat16)
    return residual_rows


def solution(mesh):
    return jax.shard_map(
        on_device,
        mesh=mesh,
        in_specs=(
            P("sp", "tp"),
            P(None, "tp"),
            P(None, "tp", "sp"),
            P(None, "tp", "sp"),
            P(None, None, "tp"),
            P(None, "tp"),
            P(None, "tp"),
            P(None, "tp"),
            P(None, "sp", "tp"),
        ),
        out_specs=P("sp", "tp"),
        check_vma=False,
    )
```

profile of v0, /device:TPU:0, one launch (start us, length us, event | category | flops | bytes accessed | tf_op | source)
XLA Modules:
  0.0 397.9 jit_solution(1611705756857018403)
XLA Ops:
  6.5 0.7 all-gather.8.cloned.1.call-update
  7.3 0.0 all-gather.6.cloned.1.call-start
  7.3 0.7 all-gather.6.cloned.1.call-update
  8.0 0.0 reduce-scatter.3.cloned.1.call-start
  8.1 1.8 fusion
  9.8 8.4 %psum.14 = f32[768]{0:T(1024)S(1)} all-reduce(f32[768]{0:T(1024)S(1)} %fusion), channel_id=1, replica_groups=mesh['sp'=8,'tp'=4] {'tp'}, use_global_device_ids=true, to_apply=%region_1.0 | all-reduce | flops 768 | bytes 6144 | tf_op jit(solution)/shard_map/psum | solution.py:24
  18.2 68.5 %all-gather.8.cloned.1.call-done = bf16[2,1024,1024]{2,1,0:T(8,128)(2,1)} async-done(((bf16[2,1024,128]{2,1,0:T(8,128)(2,1)}), bf16[2,1024,1024]{2,1,0:T(8,128)(2,1)}) %all-gather.8.cloned.1.call-update) | async-done | bytes 4194320 | tf_op jit(solution)/shard_map/all_gather | solution.py:95
  86.8 3.4 fusion.20
  90.2 71.4 %all-gather.6.cloned.1.call-done = bf16[2,1024,1024]{2,1,0:T(8,128)(2,1)} async-done(((bf16[2,1024,128]{2,1,0:T(8,128)(2,1)}), bf16[2,1024,1024]{2,1,0:T(8,128)(2,1)}) %all-gather.6.cloned.1.call-update) | async-done | bytes 4194320 | tf_op jit(solution)/shard_map/all_gather | solution.py:94
  161.7 3.4 fusion.21
  165.1 1.9 pad_maximum_fusion
  167.0 0.0 reduce-scatter.3.cloned.1.call-update
  167.1 0.0 all-gather.12.cloned.1.call-start
  167.1 0.5 all-gather.12.cloned.1.call-update
  167.6 0.0 all-gather.10.cloned.1.call-start
  167.7 0.0 copy-done.3
  167.7 0.1 copy-done.1
  167.9 35.2 %reduce-scatter.3.cloned.1.call-done = bf16[256,2,768]{0,2,1:T(8,128)(2,1)} async-done(((bf16[1024,2,768]{0,2,1:T(8,128)(2,1)}), bf16[256,2,768]{0,2,1:T(8,128)(2,1)}) %reduce-scatter.3.cloned.1.call-update) | async-done | bytes 786448 | tf_op jit(solution)/shard_map/reduce_scatter | solution.py:35
  203.1 1.2 convert_element_type.123
  204.4 0.2 fusion.99
  204.6 3.4 collective-permute-start
  208.0 1.4 collective-permute-done
  209.4 0.1 maximum_convert_fusion
  209.5 3.3 fusion.102
  212.8 0.3 multiply_reduce_fusion.1
  213.1 1.1 multiply_convert_fusion.1
  214.2 0.0 reduce-scatter.5.cloned.1.call-start
  214.3 63.7 %all-gather.12.cloned.1.call-done = bf16[2,1024,1024]{2,1,0:T(8,128)(2,1)} async-done(((bf16[2,128,1024]{2,1,0:T(8,128)(2,1)}), bf16[2,1024,1024]{2,1,0:T(8,128)(2,1)}) %all-gather.12.cloned.1.call-update) | async-done | bytes 4194320 | tf_op jit(solution)/shard_map/all_gather | solution.py:96
  278.0 19.8 %all-gather.10.cloned.1.call-done = bf16[1024,768]{0,1:T(8,128)(2,1)} async-done(((bf16[256,768]{0,1:T(8,128)(2,1)}), bf16[1024,768]{0,1:T(8,128)(2,1)}) %all-gather.10.cloned.1.call-update) | async-done | bytes 1572880 | tf_op jit(solution)/shard_map/all_gather | solution.py:71
  297.7 4.1 %fusion.4 = (f32[768]{0:T(1024)S(1)}, bf16[768,1024]{1,0:T(8,128)(2,1)S(1)}) fusion(bf16[1024,768]{0,1:T(8,128)(2,1)} %all-gather.10.cloned.1.call-done, bf16[2,1024,1024]{2,1,0:T(8,128)(2,1)} %all-gather.12.cloned.1.call-done, bf16[768,1024]{1,0:T(8,128)(2,1)S(1)} %copy-done), kind=kOutput, calls=%fused_computation.10 | convolution fusion | flops 1615330560 | bytes 6818816 | tf_op jit(solution)/shard_map/dot_general | solution.py:70
  301.8 5.9 %psum.15 = f32[768]{0:T(1024)S(1)} all-reduce(f32[768]{0:T(1024)S(1)} %get-tuple-element.81), channel_id=1, replica_groups=mesh['sp'=8,'tp'=4] {'tp'}, use_global_device_ids=true, to_apply=%region_6.7 | all-reduce | flops 768 | bytes 6144 | tf_op jit(solution)/shard_map/psum | solution.py:24
  307.7 3.6 fusion.19
  311.3 1.9 fusion.18
  313.2 2.0 pad_maximum_fusion.1
  315.2 0.0 reduce-scatter.5.cloned.1.call-update
  315.2 0.0 all-gather.14.cloned.1.call-start
  315.2 38.9 %reduce-scatter.5.cloned.1.call-done = bf16[256,2,768]{0,2,1:T(8,128)(2,1)} async-done(((bf16[1024,2,768]{0,2,1:T(8,128)(2,1)}), bf16[256,2,768]{0,2,1:T(8,128)(2,1)}) %reduce-scatter.5.cloned.1.call-update) | async-done | bytes 786448 | tf_op jit(solution)/shard_map/reduce_scatter | solution.py:35
  354.1 1.2 convert_element_type.137
  355.4 0.2 fusion.98
  355.6 3.4 collective-permute-start.1
  359.0 1.4 collective-permute-done.1
  360.4 0.1 maximum_convert_fusion.1
  360.5 3.3 fusion.100
  363.8 0.3 multiply_reduce_fusion
  364.1 1.1 multiply_convert_fusion
  365.2 0.0 all-gather.14.cloned.1.call-update
  365.2 20.8 %all-gather.14.cloned.1.call-done = bf16[1024,768]{0,1:T(8,128)(2,1)} async-done(((bf16[256,768]{0,1:T(8,128)(2,1)}), bf16[1024,768]{0,1:T(8,128)(2,1)}) %all-gather.14.cloned.1.call-update) | async-done | bytes 1572880 | tf_op jit(solution)/shard_map/all_gather | solution.py:71
  386.0 5.0 %fusion.7 = bf16[768,1024]{1,0:T(8,128)(2,1)} fusion(bf16[768,1024]{1,0:T(8,128)(2,1)S(1)} %get-tuple-element.82, bf16[1024,768]{0,1:T(8,128)(2,1)} %all-gather.14.cloned.1.call-done, bf16[2,1024,1024]{2,1,0:T(8,128)(2,1)} %all-gather.12.cloned.1.call-done), kind=kOutput, calls=%fused_computation.13 | convolution fusion | flops 1612972032 | bytes 6815744 | tf_op jit(solution)/shard_map/dot_general | solution.py:70
  (31 shorter events, 0.2 us)
Async XLA Ops:
  6.5 80.2 %copy-start = (bf16[768,1024]{1,0:T(8,128)(2,1)S(1)}, bf16[768,1024]{1,0:T(8,128)(2,1)}, u32[]{:S(2)}) copy-start(bf16[768,1024]{1,0:T(8,128)(2,1)} %param.9) | copy-start | bytes 4718596
  6.5 11.7 %copy-start.2 = (bf16[2,1024]{1,0:T(2,128)(2,1)S(1)}, bf16[2,1024]{1,0:T(2,128)(2,1)}, u32[]{:S(2)}) copy-start(bf16[2,1024]{1,0:T(2,128)(2,1)} %param.10) | copy-start | bytes 12292
  6.5 80.2 %all-gather.8.cloned.1.call-start = ((), (), s32[]{:S(2)}) async-start(), calls=%async_computation.3 | async-start | bytes 4718592 | tf_op jit(solution)/shard_map/all_gather | solution.py:95
  7.3 154.4 %all-gather.6.cloned.1.call-start = ((), (), s32[]{:S(2)}) async-start(), calls=%async_computation.2 | async-start | bytes 4718592 | tf_op jit(solution)/shard_map/all_gather | solution.py:94
  8.0 195.1 %reduce-scatter.3.cloned.1.call-start = ((), (), s32[]{:S(2)}) async-start(), calls=%async_computation.4 | async-start | bytes 3932160 | tf_op jit(solution)/shard_map/reduce_scatter | solution.py:35
  167.0 0.7 copy-start.3
  167.0 0.7 copy-start.4
  167.0 0.8 copy-start.1
  167.1 110.9 %all-gather.12.cloned.1.call-start = ((), (), s32[]{:S(2)}) async-start(), calls=%async_computation.6 | async-start | bytes 4718592 | tf_op jit(solution)/shard_map/all_gather | solution.py:96
  167.6 130.1 %all-gather.10.cloned.1.call-start = ((), (), s32[]{:S(2)}) async-start(), calls=%async_computation.5 | async-start | bytes 1966080 | tf_op jit(solution)/shard_map/all_gather | solution.py:71
  167.9 40.1 %copy-start.5 = (bf16[2,256]{1,0:T(2,128)(2,1)S(1)}, bf16[2,256]{1,0:T(2,128)(2,1)}, u32[]{:S(2)}) copy-start(bf16[2,256]{1,0:T(2,128)(2,1)} %param.16) | copy-start | bytes 3076
  204.6 4.8 %collective-permute-start = (bf16[256,30]{0,1:T(8,128)(2,1)S(1)}, bf16[256,30]{0,1:T(8,128)(2,1)S(1)}, u32[]{:S(2)}, u32[]{:S(2)}) collective-permute-start(bf16[256,30]{0,1:T(8,128)(2,1)S(1)} %slice.651), channel_id=1, source_target_pairs={{0,4},{4,8},{8,12},{12,16},{16,20},{20,24},{24,28},{1,5},{5,9},{9,... | collective-permute-start | bytes 46088 | tf_op jit(solution)/shard_map/ppermute | solution.py:19
  214.2 139.9 %reduce-scatter.5.cloned.1.call-start = ((), (), s32[]{:S(2)}) async-start(), calls=%async_computation.7 | async-start | bytes 3932160 | tf_op jit(solution)/shard_map/reduce_scatter | solution.py:35
  307.7 3.6 copy-start.6
  315.2 70.9 %all-gather.14.cloned.1.call-start = ((), (), s32[]{:S(2)}) async-start(), calls=%async_computation.8 | async-start | bytes 1966080 | tf_op jit(solution)/shard_map/all_gather | solution.py:71
  355.6 4.8 %collective-permute-start.1 = (bf16[256,30]{0,1:T(8,128)(2,1)S(1)}, bf16[256,30]{0,1:T(8,128)(2,1)S(1)}, u32[]{:S(2)}, u32[]{:S(2)}) collective-permute-start(bf16[256,30]{0,1:T(8,128)(2,1)S(1)} %slice.719), channel_id=1, source_target_pairs={{0,4},{4,8},{8,12},{12,16},{16,20},{20,24},{24,28},{1,5},{5,9},{9,... | collective-permute-start | bytes 46088 | tf_op jit(solution)/shard_map/ppermute | solution.py:19
Sparse Core Ops, SparseCore 0:
  9.4 77.3 all-gather.7
  88.8 72.8 all-gather.5
  167.2 35.8 reduce-scatter.2
  205.1 72.7 all-gather.11
  279.4 18.3 all-gather.9
  315.3 38.7 reduce-scatter.4
  365.3 20.6 all-gather.13
where the time goes:
time: 398 us
  waiting for transfers between devices  323 us (81%)
  matrix products  21.4 us (5%)
  other arithmetic  18.2 us (5%)
  blocking collectives  14.3 us (4%)
  between operations  13.7 us (3%)
  starting transfers between devices  7.01 us (2%)
    reduce_scatter x2, waiting for transfers between devices, gated_input(): lax.psum_scatter(jnp.stack([value_part, gate_part], axis=1).astype(jnp.bf...  74.1 us
    all_gather x1, waiting for transfers between devices, on_device(): lax.all_gather(value_proj, 'sp', axis=2, tiled=True)  71.4 us
    all_gather x1, waiting for transfers between devices, on_device(): lax.all_gather(gate_proj, 'sp', axis=2, tiled=True)  68.5 us
    all_gather x1, waiting for transfers between devices, on_device(): lax.all_gather(out_proj, 'sp', axis=1, tiled=True)  63.7 us
    all_gather x2, waiting for transfers between devices, project_out(): lax.all_gather(mixed, 'tp', axis=0, tiled=True)  40.6 us
    psum x2, blocking collectives, rms_normed(): squares = lax.psum(jnp.sum(wide_rows * wide_rows, axis=1), 'tp')  14.3 us
    dot_general x2, matrix products, project_out(): lax.dot_general(lax.all_gather(mixed, 'tp', axis=0, tiled=True), w_out, (...  9.1 us
  transfers between devices with their start and end apart: 9, of which 9 were waited for; matrix products, arithmetic and copies ran while one was open for 3% of the time, Pallas kernels for 0%

commit v1 on v0

--- a/solution.py
+++ b/solution.py
@@ -1,6 +1,8 @@
 import jax
 import jax.numpy as jnp
 from jax import lax
+from jax.experimental import pallas as pl
+from jax.experimental.pallas import tpu as pltpu
 from jax.sharding import PartitionSpec as P
 
 D = 4096
@@ -111,9 +113,457 @@
     return residual_rows
 
 
+MESH = pl.DeviceIdType.MESH
+HALO = 32
+ROW_TILE = 256
+CONV_TILE = 64
+VMEM_BYTES = 62 * 1024 * 1024
+
+
+def fused_kernel(
+    n_sp,
+    n_tp,
+    hidden_ref,
+    norm_ref,
+    value_ref,
+    gate_ref,
+    taps_ref,
+    bias_ref,
+    ggain_ref,
+    gshift_ref,
+    out_proj_ref,
+    out_ref,
+    w_in,
+    w_out,
+    scaled,
+    part,
+    from_core,
+    to_chip,
+    from_chip,
+    extended,
+    halo_send,
+    halo_recv,
+    mixed,
+    squares,
+    load_sem,
+    w_send,
+    w_recv,
+    t_send,
+    t_recv,
+    s_send,
+    s_recv,
+):
+    layers, width = taps_ref.shape[0], taps_ref.shape[1]
+    rows, feats = hidden_ref.shape
+    piece = value_ref.shape[2]
+    blocks = n_sp // n_tp
+    channels = blocks * piece
+    reach = width - 1
+    nz = n_sp // 2
+    s = lax.axis_index("sp")
+    t = lax.axis_index("tp")
+    z, y = s // 2, s % 2
+    chip, core = t // 2, t % 2
+    core_mate = chip * 2 + (1 - core)
+    chip_mate = (1 - chip) * 2 + core
+    far_mate = (1 - chip) * 2 + (1 - core)
+
+    loads = []
+    for level in range(layers):
+        for kind, (source, target) in enumerate(
+            (
+                (value_ref.at[level], w_in.at[level, s, :, pl.ds(0, piece)]),
+                (gate_ref.at[level], w_in.at[level, s, :, pl.ds(piece, piece)]),
+                (
+                    out_proj_ref.at[level],
+                    w_out.at[level, pl.ds(pl.multiple_of(s * piece, piece), piece), :],
+                ),
+            )
+        ):
+            copy = pltpu.make_async_copy(source, target, load_sem.at[level, kind])
+            copy.start()
+            loads.append(copy)
+
+    barrier = pltpu.get_barrier_semaphore()
+
+    def greet(sp_index, tp_index):
+        pl.semaphore_signal(barrier, inc=1, device_id=(sp_index, tp_index), device_id_type=MESH)
+
+    up, down = z < nz - 1, z > 0
+    corner_up = jnp.logical_and(up, y == 1)
+    corner_down = jnp.logical_and(down, y == 0)
+    for mate in (core_mate, chip_mate, far_mate):
+        greet(s, mate)
+    greet(z * 2 + 1 - y, t)
+    for condition, target in (
+        (up, s + 2),
+        (down, s - 2),
+        (corner_up, s + 1),
+        (corner_down, s - 1),
+    ):
+
+        @pl.when(condition)
+        def _(target=target):
+            greet(target, t)
+
+    mates = 4
+    for condition in (up, down, corner_up, corner_down):
+        mates = mates + condition.astype(jnp.int32)
+    pl.semaphore_wait(barrier, mates)
+
+    for copy in loads:
+        copy.wait()
+
+    half = feats // 2
+    phases = []
+    for level in range(layers):
+        phases += [("in", level, 0), ("in", level, 1), ("out", level, 0)]
+
+    def chunk(phase, owner):
+        kind, level, part_index = phases[phase]
+        if kind == "in":
+            return w_in.at[level, owner, pl.ds(part_index * half, half), :]
+        return w_out.at[level, pl.ds(pl.multiple_of(owner * piece, piece), piece), :]
+
+    def weight_copy(phase, owner, way):
+        target = (s + 2, s - 2, z * 2 + 1 - y)[way]
+        return pltpu.make_async_remote_copy(
+            src_ref=chunk(phase, owner),
+            dst_ref=chunk(phase, owner),
+            send_sem=w_send.at[phase, way, owner],
+            recv_sem=w_recv.at[phase, owner],
+            device_id=(target, t),
+            device_id_type=MESH,
+        )
+
+    def own(phase):
+        @pl.when(up)
+        def _():
+            weight_copy(phase, s, 0).start()
+
+        @pl.when(down)
+        def _():
+            weight_copy(phase, s, 1).start()
+
+        weight_copy(phase, s, 2).start()
+
+    def hops(phase):
+        for hop in range(1, nz):
+
+            @pl.when(z >= hop)
+            def _(hop=hop):
+                owner = s - 2 * hop
+                weight_copy(phase, owner, 0).wait_recv()
+
+                @pl.when(up)
+                def _():
+                    weight_copy(phase, owner, 0).start()
+
+                weight_copy(phase, owner, 2).start()
+
+            @pl.when(z + hop < nz)
+            def _(hop=hop):
+                owner = s + 2 * hop
+                weight_copy(phase, owner, 1).wait_recv()
+
+                @pl.when(down)
+                def _():
+                    weight_copy(phase, owner, 1).start()
+
+                weight_copy(phase, owner, 2).start()
+
+    def crossed(phase):
+        for z_from in range(nz):
+            weight_copy(phase, z_from * 2 + 1 - y, 2).wait_recv()
+
+    def sent(phase):
+        for z_from in range(nz):
+            owner = z_from * 2 + y
+
+            @pl.when(jnp.logical_and(z >= z_from, up))
+            def _(owner=owner):
+                weight_copy(phase, owner, 0).wait_send()
+
+            @pl.when(jnp.logical_and(z <= z_from, down))
+            def _(owner=owner):
+                weight_copy(phase, owner, 1).wait_send()
+
+            weight_copy(phase, owner, 2).wait_send()
+
+    def tp_copy(level, slot, source, target, mate, sp_index=None):
+        return pltpu.make_async_remote_copy(
+            src_ref=source,
+            dst_ref=target,
+            send_sem=t_send.at[level, slot],
+            recv_sem=t_recv.at[level, slot],
+            device_id=(s if sp_index is None else sp_index, mate),
+            device_id_type=MESH,
+        )
+
+    def prepare(level):
+        gain = norm_ref[pl.ds(level, 1), :].astype(jnp.float32)
+        ones = jnp.ones((8, feats), jnp.bfloat16)
+        numbers = (((1,), (1,)), ((), ()))
+        source = hidden_ref if level == 0 else out_ref
+        for tile in range(rows // ROW_TILE):
+            span = pl.ds(tile * ROW_TILE, ROW_TILE)
+            wide = source[span, :].astype(jnp.float32)
+            scaled[span, :] = (wide * gain).astype(jnp.bfloat16)
+            square = wide * wide
+            high = square.astype(jnp.bfloat16)
+            low = (square - high.astype(jnp.float32)).astype(jnp.bfloat16)
+            total = lax.dot_general(ones, high, numbers, preferred_element_type=jnp.float32)
+            total = total + lax.dot_general(ones, low, numbers, preferred_element_type=jnp.float32)
+            squares[level, t, :, span] = total
+        for slot, mate in enumerate((core_mate, chip_mate, far_mate)):
+            square_copy(level, slot, mate).start()
+
+    def square_copy(level, slot, mate):
+        return pltpu.make_async_remote_copy(
+            src_ref=squares.at[level, t],
+            dst_ref=squares.at[level, t],
+            send_sem=s_send.at[level, slot],
+            recv_sem=s_recv.at[level, slot],
+            device_id=(s, mate),
+            device_id_type=MESH,
+        )
+
+    def row_scales(level):
+        for slot, mate in enumerate((core_mate, chip_mate, far_mate)):
+            copy = square_copy(level, slot, mate)
+            copy.wait_send()
+            copy.wait_recv()
+        total = squares[level, 0]
+        for index in range(1, n_tp):
+            total = total + squares[level, index]
+        scale = lax.rsqrt(total / D + row_floor)
+        return scale.T[:, 0:1]
+
+    def products(level, owner):
+        @pl.loop(0, blocks * (rows // ROW_TILE))
+        def _(step):
+            block = step // (rows // ROW_TILE)
+            tile = step % (rows // ROW_TILE)
+            span = pl.ds(pl.multiple_of(tile * ROW_TILE, ROW_TILE), ROW_TILE)
+            part[owner, block, span, :] = jnp.dot(
+                scaled[span, :],
+                w_in[level, owner * blocks + block],
+                preferred_element_type=jnp.float32,
+            ).astype(jnp.bfloat16)
+
+    base = 2 + blocks
+
+    def core_copy(level, slot):
+        owner = (far_mate, core_mate)[slot]
+        return tp_copy(level, slot, part.at[owner], from_core.at[level, slot], core_mate)
+
+    def chip_copy(level, block):
+        return tp_copy(
+            level, 2 + block, to_chip.at[block], from_chip.at[level, block], chip_mate
+        )
+
+    def halo_copy(level):
+        return tp_copy(level, base + 3, halo_send, halo_recv.at[level], t, s + 1)
+
+    def mixed_copy(level, slot):
+        owner = (t, t, chip_mate)[slot]
+        mate = (core_mate, chip_mate, core_mate)[slot]
+        return tp_copy(
+            level, base + slot, mixed.at[level, owner], mixed.at[level, owner], mate
+        )
+
+    def first_half(level):
+        products(level, far_mate)
+        core_copy(level, 0).start()
+        products(level, chip_mate)
+        core_copy(level, 0).wait_recv()
+        for block in range(blocks):
+            to_chip[block] = (
+                part[chip_mate, block].astype(jnp.float32)
+                + from_core[level, 0, block].astype(jnp.float32)
+            ).astype(jnp.bfloat16)
+            chip_copy(level, block).start()
+        products(level, core_mate)
+        core_copy(level, 1).start()
+        products(level, t)
+        core_copy(level, 1).wait_recv()
+
+    def gating(level):
+        scale = row_scales(level)
+        for block in range(blocks):
+            lanes = pl.ds(block * piece, piece)
+            chip_copy(level, block).wait_recv()
+            total = (
+                part[t, block].astype(jnp.float32)
+                + from_core[level, 1, block].astype(jnp.float32)
+                + from_chip[level, block].astype(jnp.float32)
+            ) * scale
+            gated = (total[:, :piece] * jax.nn.sigmoid(total[:, piece:])).astype(jnp.bfloat16)
+            halo_send[:, lanes] = gated[rows - HALO :]
+            extended[pl.ds(HALO, rows), lanes] = gated.astype(jnp.float32)
+
+        @pl.when(s < n_sp - 1)
+        def _():
+            halo_copy(level).start()
+
+    def filtering(level):
+        taps = taps_ref[level].astype(jnp.float32)
+        bias = bias_ref[pl.ds(level, 1), :].astype(jnp.float32)
+        ggain = ggain_ref[pl.ds(level, 1), :].astype(jnp.float32)
+        gshift = gshift_ref[pl.ds(level, 1), :].astype(jnp.float32)
+
+        @pl.when(s > 0)
+        def _():
+            halo_copy(level).wait_recv()
+            extended[pl.ds(0, HALO), :] = halo_recv[level].astype(jnp.float32)
+
+        @pl.when(s == 0)
+        def _():
+            extended[pl.ds(0, HALO), :] = jnp.zeros((HALO, channels), jnp.float32)
+
+        @pl.loop(0, rows // CONV_TILE)
+        def _(tile):
+            start = pl.multiple_of(tile * CONV_TILE, CONV_TILE)
+            window = extended[pl.ds(start, CONV_TILE + HALO), :]
+            filtered = jnp.zeros((CONV_TILE, channels), jnp.float32) + bias
+            for offset in range(width):
+                low = HALO - reach + offset
+                filtered = filtered + taps[offset : offset + 1, :] * window[low : low + CONV_TILE]
+            mean = jnp.mean(filtered, axis=1, keepdims=True)
+            centered = filtered - mean
+            var = jnp.mean(centered * centered, axis=1, keepdims=True)
+            normed = centered * lax.rsqrt(var + group_floor) * ggain + gshift
+            mixed[level, t, pl.ds(start, CONV_TILE), :] = (
+                normed * jax.nn.sigmoid(normed)
+            ).astype(jnp.bfloat16)
+
+        mixed_copy(level, 1).start()
+        mixed_copy(level, 0).start()
+
+    def relay(level):
+        mixed_copy(level, 1).wait_recv()
+        mixed_copy(level, 2).start()
+
+    def projecting(level):
+        mixed_copy(level, 0).wait_recv()
+        mixed_copy(level, 2).wait_recv()
+        source = hidden_ref if level == 0 else out_ref
+        tiles = rows // ROW_TILE
+
+        @pl.loop(0, tiles)
+        def _(tile):
+            span = pl.ds(pl.multiple_of(tile * ROW_TILE, ROW_TILE), ROW_TILE)
+            total = source[span, :].astype(jnp.float32)
+            for owner in range(n_tp):
+                total = total + jnp.dot(
+                    mixed[level, owner, span, :],
+                    w_out[level, pl.ds(owner * channels, channels), :],
+                    preferred_element_type=jnp.float32,
+                )
+            out_ref[span, :] = total.astype(jnp.bfloat16)
+
+    def settle(level):
+        for slot in range(2):
+            core_copy(level, slot).wait_send()
+        for block in range(blocks):
+            chip_copy(level, block).wait_send()
+        for slot in range(3):
+            mixed_copy(level, slot).wait_send()
+
+        @pl.when(s < n_sp - 1)
+        def _():
+            halo_copy(level).wait_send()
+
+    own(0)
+    own(1)
+    prepare(0)
+    for level in range(layers):
+        first = 3 * level
+        last = level == layers - 1
+        if level == 0:
+            hops(0)
+            own(2)
+            hops(1)
+            if not last:
+                own(3)
+        crossed(first)
+        crossed(first + 1)
+        first_half(level)
+        hops(first + 2)
+        if not last:
+            own(first + 4)
+        gating(level)
+        filtering(level)
+        if not last:
+            hops(first + 3)
+            own(first + 5)
+        relay(level)
+        crossed(first + 2)
+        projecting(level)
+        settle(level)
+        if not last:
+            prepare(level + 1)
+            hops(first + 4)
+    for phase in range(len(phases)):
+        sent(phase)
+
+
+def fused(n_sp, n_tp, *arrays):
+    hidden_in, norm_gain, value_proj = arrays[:3]
+    rows, feats = hidden_in.shape
+    layers = norm_gain.shape[0]
+    piece = value_proj.shape[2]
+    blocks = n_sp // n_tp
+    channels = blocks * piece
+    kinds = 3
+    vmem = pl.BlockSpec(memory_space=pltpu.VMEM)
+    hbm = pl.BlockSpec(memory_space=pl.ANY)
+    low, wide = jnp.bfloat16, jnp.float32
+    slots = 2 + blocks + 4
+    return pl.pallas_call(
+        lambda *refs: fused_kernel(n_sp, n_tp, *refs),
+        out_shape=jax.ShapeDtypeStruct((rows, feats), low),
+        in_specs=[vmem, vmem, hbm, hbm, vmem, vmem, vmem, vmem, hbm],
+        out_specs=vmem,
+        scratch_shapes=[
+            pltpu.VMEM((layers, n_sp, feats, 2 * piece), low),
+            pltpu.VMEM((layers, n_sp * piece, feats), low),
+            pltpu.VMEM((rows, feats), low),
+            pltpu.VMEM((n_tp, blocks, rows, 2 * piece), low),
+            pltpu.VMEM((layers, 2, blocks, rows, 2 * piece), low),
+            pltpu.VMEM((blocks, rows, 2 * piece), low),
+            pltpu.VMEM((layers, blocks, rows, 2 * piece), low),
+            pltpu.VMEM((HALO + rows, channels), wide),
+            pltpu.VMEM((HALO, channels), low),
+            pltpu.VMEM((layers, HALO, channels), low),
+            pltpu.VMEM((layers, n_tp, rows, channels), low),
+            pltpu.VMEM((layers, n_tp, 8, rows), wide),
+            pltpu.SemaphoreType.DMA((layers, kinds)),
+            pltpu.SemaphoreType.DMA((layers * kinds, 3, n_sp)),
+            pltpu.SemaphoreType.DMA((layers * kinds, n_sp)),
+            pltpu.SemaphoreType.DMA((layers, slots)),
+            pltpu.SemaphoreType.DMA((layers, slots)),
+            pltpu.SemaphoreType.DMA((layers, 3)),
+            pltpu.SemaphoreType.DMA((layers, 3)),
+        ],
+        compiler_params=pltpu.CompilerParams(
+            collective_id=0, has_side_effects=True, vmem_limit_bytes=VMEM_BYTES
+        ),
+    )(*arrays)
+
+
 def solution(mesh):
+    n_sp, n_tp = mesh.shape["sp"], mesh.shape["tp"]
+    piece = C // n_sp
+    small = n_tp == 4 and GROUPS == n_tp and n_sp % n_tp == 0 and piece % 128 == 0
+
+    def local(*arrays):
+        if small and arrays[0].shape[0] % ROW_TILE == 0:
+            return fused(n_sp, n_tp, *arrays)
+        return on_device(*arrays)
+
     return jax.shard_map(
-        on_device,
+        local,
         mesh=mesh,
         in_specs=(
             P("sp", "tp"),

time: 398 us -> 196 us (0.49)
  waiting for transfers between devices: 323 us -> 0 us
  Pallas kernels: 0 us -> 189 us
  matrix products: 21.4 us -> 0 us
  other arithmetic: 18.2 us -> 0 us
  blocking collectives: 14.3 us -> 0 us
  between operations: 13.7 us -> 0.01 us
  starting transfers between devices: 7.01 us -> 0 us
    all_gather x5 -> x0, waiting for transfers between devices: 244 us -> none  [the longest x1 71.4 us: on_device(): lax.all_gather(value_proj, 'sp', axis=2, tiled=True)]
    pallas_call x0 -> x1, Pallas kernels: none -> 189 us  [fused(): pl.pallas_call(lambda *refs: fused_kernel(n_sp, n_tp, *refs), out_shape=j...]
    reduce_scatter x2 -> x0, waiting for transfers between devices: 74.1 us -> none  [gated_input(): lax.psum_scatter(jnp.stack([value_part, gate_part], axis=1).astype(jnp.bf...]
    dot_general x6 -> x0, matrix products: 21.4 us -> none  [the longest x2 9.1 us: project_out(): lax.dot_general(lax.all_gather(mixed, 'tp', axis=0, tiled=True), w_out, (...]
    psum x2 -> x0, blocking collectives: 14.3 us -> none  [rms_normed(): squares = lax.psum(jnp.sum(wide_rows * wide_rows, axis=1), 'tp')]
    reduce_sum x5 -> x0, other arithmetic: 8.91 us -> none  [the longest x2 6.54 us: group_normed(): group_mean = jnp.mean(grouped, axis=1, keepdims=True)]
    ppermute x2 -> x0, starting transfers between devices: 6.77 us -> none  [passed_along(): lax.ppermute(value, axis, [(source, source + steps) for source in range(i...]
    convert_element_type x12 -> x0, other arithmetic: 5.34 us -> none  [the longest x2 2.5 us: gated_input(): summed = lax.psum_scatter(jnp.stack([value_part, gate_part], axis=1).asty...]
  transfers between devices with their start and end apart: 9 -> 0, of which waited for: 9 -> 0; matrix products, arithmetic and copies ran while one was open for 3% -> 0% of each run, Pallas kernels for 0% -> 0%
where the time goes in v1:
time: 196 us; the launch traced here: 193 us
  Pallas kernels  189 us (96%)
  local copies, waits for them, and re-layouts  4.04 us (2%)
    pallas_call x1, Pallas kernels, fused(): pl.pallas_call(lambda *refs: fused_kernel(n_sp, n_tp, *refs), out_shape=j...  189 us
    unnamed x2, local copies, waits for them, and re-layouts  4.04 us

profile of v1, /device:TPU:0, one launch (start us, length us, event | category | flops | bytes accessed | tf_op | source)
XLA Modules:
  0.0 192.7 jit_solution(13317506796714099800)
XLA Ops:
  0.0 1.4 copy.10.refs_4_
  1.4 188.6 %shard_map.91 = bf16[768,1024]{1,0:T(8,128)(2,1)} custom-call(bf16[768,1024]{1,0:T(8,128)(2,1)} %refs_0_.1, bf16[2,1024]{1,0:T(2,128)(2,1)} %refs_1_.1, bf16[2,1024,128]{2,1,0:T(8,128)(2,1)} %refs_2_.1, bf16[2,1024,128]{2,1,0:T(8,128)(2,1)} %refs_3_.1, bf16[2,31,256]{2,1,0:T(8,128)(2,1)} %copy.10.refs_4_, bf16[2,256]{1,0:T(2,128)(2,1)} %refs_5_.1, ...), custom_call_target="tpu_custom_call" | custom-call | tf_op jit(solution)/shard_map/pallas_call | solution.py:523
  190.0 2.7 %copy.12 = bf16[768,1024]{1,0:T(8,128)(2,1)} copy(bf16[768,1024]{1,0:T(8,128)(2,1)} %shard_map.91) | data formatting | bytes 3145728

commit v2 on v1

--- a/solution.py
+++ b/solution.py
@@ -118,6 +118,7 @@
 ROW_TILE = 256
 CONV_TILE = 64
 VMEM_BYTES = 62 * 1024 * 1024
+SPLIT = 3
 
 
 def fused_kernel(
@@ -219,76 +220,91 @@
     for level in range(layers):
         phases += [("in", level, 0), ("in", level, 1), ("out", level, 0)]
 
-    def chunk(phase, owner):
+    def chunk(phase, owner, lot):
         kind, level, part_index = phases[phase]
+        deep = half if kind == "in" else piece
+        cut = deep - deep * SPLIT // 16 // 16 * 16
+        low, size = (0, cut) if lot == 0 else (cut, deep - cut)
         if kind == "in":
-            return w_in.at[level, owner, pl.ds(part_index * half, half), :]
-        return w_out.at[level, pl.ds(pl.multiple_of(owner * piece, piece), piece), :]
-
-    def weight_copy(phase, owner, way):
+            return w_in.at[level, owner, pl.ds(part_index * half + low, size), :]
+        return w_out.at[level, pl.ds(pl.multiple_of(owner * piece, piece) + low, size), :]
+
+    def weight_copy(phase, owner, way, lot):
         target = (s + 2, s - 2, z * 2 + 1 - y)[way]
         return pltpu.make_async_remote_copy(
-            src_ref=chunk(phase, owner),
-            dst_ref=chunk(phase, owner),
-            send_sem=w_send.at[phase, way, owner],
-            recv_sem=w_recv.at[phase, owner],
+            src_ref=chunk(phase, owner, lot),
+            dst_ref=chunk(phase, owner, lot),
+            send_sem=w_send.at[phase, lot, way, owner],
+            recv_sem=w_recv.at[phase, lot, owner],
             device_id=(target, t),
             device_id_type=MESH,
         )
 
-    def own(phase):
+    def both_ways(phase, owner, lot):
         @pl.when(up)
         def _():
-            weight_copy(phase, s, 0).start()
+            weight_copy(phase, owner, 0, lot).start()
 
         @pl.when(down)
         def _():
-            weight_copy(phase, s, 1).start()
-
-        weight_copy(phase, s, 2).start()
+            weight_copy(phase, owner, 1, lot).start()
+
+    def own(phase):
+        for lot in (1, 0):
+            weight_copy(phase, s, 2, lot).start()
+            both_ways(phase, s, lot)
 
     def hops(phase):
+        across = z * 2 + 1 - y
+        weight_copy(phase, across, 2, 1).wait_recv()
+        both_ways(phase, across, 1)
+        moves = ((y, 1), (y, 0), (1 - y, 1))
         for hop in range(1, nz):
-
-            @pl.when(z >= hop)
-            def _(hop=hop):
-                owner = s - 2 * hop
-                weight_copy(phase, owner, 0).wait_recv()
-
-                @pl.when(up)
-                def _():
-                    weight_copy(phase, owner, 0).start()
-
-                weight_copy(phase, owner, 2).start()
-
-            @pl.when(z + hop < nz)
-            def _(hop=hop):
-                owner = s + 2 * hop
-                weight_copy(phase, owner, 1).wait_recv()
-
-                @pl.when(down)
-                def _():
-                    weight_copy(phase, owner, 1).start()
-
-                weight_copy(phase, owner, 2).start()
+            for column, lot in moves:
+
+                @pl.when(z >= hop)
+                def _(hop=hop, column=column, lot=lot):
+                    owner = (z - hop) * 2 + column
+                    weight_copy(phase, owner, 0, lot).wait_recv()
+
+                    @pl.when(up)
+                    def _():
+                        weight_copy(phase, owner, 0, lot).start()
+
+                    if lot == 0:
+                        weight_copy(phase, owner, 2, lot).start()
+
+                @pl.when(z + hop < nz)
+                def _(hop=hop, column=column, lot=lot):
+                    owner = (z + hop) * 2 + column
+                    weight_copy(phase, owner, 1, lot).wait_recv()
+
+                    @pl.when(down)
+                    def _():
+                        weight_copy(phase, owner, 1, lot).start()
+
+                    if lot == 0:
+                        weight_copy(phase, owner, 2, lot).start()
 
     def crossed(phase):
         for z_from in range(nz):
-            weight_copy(phase, z_from * 2 + 1 - y, 2).wait_recv()
+            weight_copy(phase, z_from * 2 + 1 - y, 2, 0).wait_recv()
 
     def sent(phase):
         for z_from in range(nz):
-            owner = z_from * 2 + y
-
-            @pl.when(jnp.logical_and(z >= z_from, up))
-            def _(owner=owner):
-                weight_copy(phase, owner, 0).wait_send()
-
-            @pl.when(jnp.logical_and(z <= z_from, down))
-            def _(owner=owner):
-                weight_copy(phase, owner, 1).wait_send()
-
-            weight_copy(phase, owner, 2).wait_send()
+            for column, lot in ((y, 0), (y, 1), (1 - y, 1)):
+                owner = z_from * 2 + column
+
+                @pl.when(jnp.logical_and(z >= z_from, up))
+                def _(owner=owner, lot=lot):
+                    weight_copy(phase, owner, 0, lot).wait_send()
+
+                @pl.when(jnp.logical_and(z <= z_from, down))
+                def _(owner=owner, lot=lot):
+                    weight_copy(phase, owner, 1, lot).wait_send()
+
+            weight_copy(phase, z_from * 2 + y, 2, 0).wait_send()
+        weight_copy(phase, s, 2, 1).wait_send()
 
     def tp_copy(level, slot, source, target, mate, sp_index=None):
         return pltpu.make_async_remote_copy(
@@ -490,12 +506,13 @@
         crossed(first + 1)
         first_half(level)
         hops(first + 2)
+        gating(level)
         if not last:
+            hops(first + 3)
             own(first + 4)
-        gating(level)
         filtering(level)
         if not last:
-            hops(first + 3)
+            hops(first + 4)
             own(first + 5)
         relay(level)
         crossed(first + 2)
@@ -503,7 +520,6 @@
         settle(level)
         if not last:
             prepare(level + 1)
-            hops(first + 4)
     for phase in range(len(phases)):
         sent(phase)
 
@@ -539,8 +555,8 @@
             pltpu.VMEM((layers, n_tp, rows, channels), low),
             pltpu.VMEM((layers, n_tp, 8, rows), wide),
             pltpu.SemaphoreType.DMA((layers, kinds)),
-            pltpu.SemaphoreType.DMA((layers * kinds, 3, n_sp)),
-            pltpu.SemaphoreType.DMA((layers * kinds, n_sp)),
+            pltpu.SemaphoreType.DMA((layers * kinds, 2, 3, n_sp)),
+            pltpu.SemaphoreType.DMA((layers * kinds, 2, n_sp)),
             pltpu.SemaphoreType.DMA((layers, slots)),
             pltpu.SemaphoreType.DMA((layers, slots)),
             pltpu.SemaphoreType.DMA((layers, 3)),

time: 196 us -> 175 us (0.89)
  Pallas kernels: 189 us -> 169 us
    pallas_call x1, Pallas kernels: 189 us -> 169 us  [fused(): pl.pallas_call(lambda *refs: fused_kernel(n_sp, n_tp, *refs), out_shape=j...]
where the time goes in v2:
time: 175 us; the launch traced here: 173 us
  Pallas kernels  169 us (97%)
  local copies, waits for them, and re-layouts  4.04 us (2%)
    pallas_call x1, Pallas kernels, fused(): pl.pallas_call(lambda *refs: fused_kernel(n_sp, n_tp, *refs), out_shape=j...  169 us
    unnamed x2, local copies, waits for them, and re-layouts  4.04 us

profile of v2, /device:TPU:0, one launch (start us, length us, event | category | flops | bytes accessed | tf_op | source)
XLA Modules:
  0.0 172.7 jit_solution(9113406184192037879)
XLA Ops:
  0.0 1.4 copy.10.refs_4_
  1.4 168.6 %shard_map.91 = bf16[768,1024]{1,0:T(8,128)(2,1)} custom-call(bf16[768,1024]{1,0:T(8,128)(2,1)} %refs_0_.1, bf16[2,1024]{1,0:T(2,128)(2,1)} %refs_1_.1, bf16[2,1024,128]{2,1,0:T(8,128)(2,1)} %refs_2_.1, bf16[2,1024,128]{2,1,0:T(8,128)(2,1)} %refs_3_.1, bf16[2,31,256]{2,1,0:T(8,128)(2,1)} %copy.10.refs_4_, bf16[2,256]{1,0:T(2,128)(2,1)} %refs_5_.1, ...), custom_call_target="tpu_custom_call" | custom-call | tf_op jit(solution)/shard_map/pallas_call | solution.py:539
  170.0 2.7 %copy.12 = bf16[768,1024]{1,0:T(8,128)(2,1)} copy(bf16[768,1024]{1,0:T(8,128)(2,1)} %shard_map.91) | data formatting | bytes 3145728

commit v3 on v2

--- a/solution.py
+++ b/solution.py
@@ -368,6 +368,8 @@
             ).astype(jnp.bfloat16)
 
     base = 2 + blocks
+    parts = rows // ROW_TILE
+    order = tuple(reversed(range(parts)))
 
     def core_copy(level, slot):
         owner = (far_mate, core_mate)[slot]
@@ -379,14 +381,13 @@
         )
 
     def halo_copy(level):
-        return tp_copy(level, base + 3, halo_send, halo_recv.at[level], t, s + 1)
-
-    def mixed_copy(level, slot):
+        return tp_copy(level, base + 3 * parts, halo_send, halo_recv.at[level], t, s + 1)
+
+    def mixed_copy(level, slot, third):
         owner = (t, t, chip_mate)[slot]
         mate = (core_mate, chip_mate, core_mate)[slot]
-        return tp_copy(
-            level, base + slot, mixed.at[level, owner], mixed.at[level, owner], mate
-        )
+        block = mixed.at[level, owner, pl.ds(third * ROW_TILE, ROW_TILE), :]
+        return tp_copy(level, base + slot * parts + third, block, block, mate)
 
     def first_half(level):
         products(level, far_mate)
@@ -428,55 +429,54 @@
         ggain = ggain_ref[pl.ds(level, 1), :].astype(jnp.float32)
         gshift = gshift_ref[pl.ds(level, 1), :].astype(jnp.float32)
 
-        @pl.when(s > 0)
-        def _():
-            halo_copy(level).wait_recv()
-            extended[pl.ds(0, HALO), :] = halo_recv[level].astype(jnp.float32)
-
-        @pl.when(s == 0)
-        def _():
-            extended[pl.ds(0, HALO), :] = jnp.zeros((HALO, channels), jnp.float32)
-
-        @pl.loop(0, rows // CONV_TILE)
-        def _(tile):
-            start = pl.multiple_of(tile * CONV_TILE, CONV_TILE)
-            window = extended[pl.ds(start, CONV_TILE + HALO), :]
-            filtered = jnp.zeros((CONV_TILE, channels), jnp.float32) + bias
-            for offset in range(width):
-                low = HALO - reach + offset
-                filtered = filtered + taps[offset : offset + 1, :] * window[low : low + CONV_TILE]
-            mean = jnp.mean(filtered, axis=1, keepdims=True)
-            centered = filtered - mean
-            var = jnp.mean(centered * centered, axis=1, keepdims=True)
-            normed = centered * lax.rsqrt(var + group_floor) * ggain + gshift
-            mixed[level, t, pl.ds(start, CONV_TILE), :] = (
-                normed * jax.nn.sigmoid(normed)
-            ).astype(jnp.bfloat16)
-
-        mixed_copy(level, 1).start()
-        mixed_copy(level, 0).start()
-
-    def relay(level):
-        mixed_copy(level, 1).wait_recv()
-        mixed_copy(level, 2).start()
-
-    def projecting(level):
-        mixed_copy(level, 0).wait_recv()
-        mixed_copy(level, 2).wait_recv()
+        per_part = ROW_TILE // CONV_TILE
+        for third in order:
+            if third == 0:
+                @pl.when(s > 0)
+                def _():
+                    halo_copy(level).wait_recv()
+                    extended[pl.ds(0, HALO), :] = halo_recv[level].astype(jnp.float32)
+
+                @pl.when(s == 0)
+                def _():
+                    extended[pl.ds(0, HALO), :] = jnp.zeros((HALO, channels), jnp.float32)
+
+            @pl.loop(third * per_part, (third + 1) * per_part)
+            def _(tile):
+                start = pl.multiple_of(tile * CONV_TILE, CONV_TILE)
+                window = extended[pl.ds(start, CONV_TILE + HALO), :]
+                filtered = jnp.zeros((CONV_TILE, channels), jnp.float32) + bias
+                for offset in range(width):
+                    low = HALO - reach + offset
+                    filtered = filtered + taps[offset : offset + 1, :] * window[low : low + CONV_TILE]
+                mean = jnp.mean(filtered, axis=1, keepdims=True)
+                centered = filtered - mean
+                var = jnp.mean(centered * centered, axis=1, keepdims=True)
+                normed = centered * lax.rsqrt(var + group_floor) * ggain + gshift
+                mixed[level, t, pl.ds(start, CONV_TILE), :] = (
+                    normed * jax.nn.sigmoid(normed)
+                ).astype(jnp.bfloat16)
+
+            mixed_copy(level, 1, third).start()
+            mixed_copy(level, 0, third).start()
+
+    def relay(level, third):
+        mixed_copy(level, 1, third).wait_recv()
+        mixed_copy(level, 2, third).start()
+
+    def projecting(level, third):
+        mixed_copy(level, 0, third).wait_recv()
+        mixed_copy(level, 2, third).wait_recv()
         source = hidden_ref if level == 0 else out_ref
-        tiles = rows // ROW_TILE
-
-        @pl.loop(0, tiles)
-        def _(tile):
-            span = pl.ds(pl.multiple_of(tile * ROW_TILE, ROW_TILE), ROW_TILE)
-            total = source[span, :].astype(jnp.float32)
-            for owner in range(n_tp):
-                total = total + jnp.dot(
-                    mixed[level, owner, span, :],
-                    w_out[level, pl.ds(owner * channels, channels), :],
-                    preferred_element_type=jnp.float32,
-                )
-            out_ref[span, :] = total.astype(jnp.bfloat16)
+        span = pl.ds(third * ROW_TILE, ROW_TILE)
+        total = source[span, :].astype(jnp.float32)
+        for owner in range(n_tp):
+            total = total + jnp.dot(
+                mixed[level, owner, span, :],
+                w_out[level, pl.ds(owner * channels, channels), :],
+                preferred_element_type=jnp.float32,
+            )
+        out_ref[span, :] = total.astype(jnp.bfloat16)
 
     def settle(level):
         for slot in range(2):
@@ -484,7 +484,8 @@
         for block in range(blocks):
             chip_copy(level, block).wait_send()
         for slot in range(3):
-            mixed_copy(level, slot).wait_send()
+            for third in order:
+                mixed_copy(level, slot, third).wait_send()
 
         @pl.when(s < n_sp - 1)
         def _():
@@ -514,9 +515,12 @@
         if not last:
             hops(first + 4)
             own(first + 5)
-        relay(level)
+        relay(level, order[0])
         crossed(first + 2)
-        projecting(level)
+        for index in range(1, parts):
+            relay(level, order[index])
+            projecting(level, order[index - 1])
+        projecting(level, order[-1])
         settle(level)
         if not last:
             prepare(level + 1)
@@ -535,7 +539,7 @@
     vmem = pl.BlockSpec(memory_space=pltpu.VMEM)
     hbm = pl.BlockSpec(memory_space=pl.ANY)
     low, wide = jnp.bfloat16, jnp.float32
-    slots = 2 + blocks + 4
+    slots = 2 + blocks + 3 * (rows // ROW_TILE) + 1
     return pl.pallas_call(
         lambda *refs: fused_kernel(n_sp, n_tp, *refs),
         out_shape=jax.ShapeDtypeStruct((rows, feats), low),

time: 175 us -> 169 us (0.966)
  Pallas kernels: 169 us -> 164 us
    pallas_call x1, Pallas kernels: 169 us -> 164 us  [fused(): pl.pallas_call(lambda *refs: fused_kernel(n_sp, n_tp, *refs), out_shape=j...]
where the time goes in v3:
time: 169 us; the launch traced here: 168 us
  Pallas kernels  164 us (97%)
  local copies, waits for them, and re-layouts  4.04 us (2%)
    pallas_call x1, Pallas kernels, fused(): pl.pallas_call(lambda *refs: fused_kernel(n_sp, n_tp, *refs), out_shape=j...  164 us
    unnamed x2, local copies, waits for them, and re-layouts  4.04 us

profile of v3, /device:TPU:0, one launch (start us, length us, event | category | flops | bytes accessed | tf_op | source)
XLA Modules:
  0.0 168.2 jit_solution(15629391575579319339)
XLA Ops:
  0.0 1.4 copy.10.refs_4_
  1.4 164.2 %shard_map.91 = bf16[768,1024]{1,0:T(8,128)(2,1)} custom-call(bf16[768,1024]{1,0:T(8,128)(2,1)} %refs_0_.1, bf16[2,1024]{1,0:T(2,128)(2,1)} %refs_1_.1, bf16[2,1024,128]{2,1,0:T(8,128)(2,1)} %refs_2_.1, bf16[2,1024,128]{2,1,0:T(8,128)(2,1)} %refs_3_.1, bf16[2,31,256]{2,1,0:T(8,128)(2,1)} %copy.10.refs_4_, bf16[2,256]{1,0:T(2,128)(2,1)} %refs_5_.1, ...), custom_call_target="tpu_custom_call" | custom-call | tf_op jit(solution)/shard_map/pallas_call | solution.py:543
  165.6 2.7 %copy.12 = bf16[768,1024]{1,0:T(8,128)(2,1)} copy(bf16[768,1024]{1,0:T(8,128)(2,1)} %shard_map.91) | data formatting | bytes 3145728
